TPU v7x, 32 devices: a whole 2x2x4 slice. The times are simulated.
32 devices in a mesh: ra: 8 (over z, y), cb: 4 (over x, core).
Axes of the slice: x: 2, y: 2, z: 4, core: 2. Of those that a mesh axis runs over, the one named last changes fastest.
Arguments:
- tokens: bfloat16 [256, 3072], P(None, 'ra'), may hold values from -8 to 8, as said below
- first_gain: float32 [3072], P('ra'), may hold values from 0.1 to 1.9
- first_gate: float32 [3072, 8192], P('ra', 'cb'), may hold values from -0.109375 to 0.109375
- first_up: float32 [3072, 8192], P('ra', 'cb'), may hold values from -0.109375 to 0.109375
- first_down: float32 [8192, 3072], P('cb', 'ra'), may hold values from -0.0625 to 0.0625
- first_gate_scale: float32 [8192], P('cb'), may hold values from 0.5 to 2
- first_up_scale: float32 [8192], P('cb'), may hold values from 0.5 to 2
- first_down_scale: float32 [3072], P('ra'), may hold values from 0.5 to 2
- second_gain: float32 [3072], P('ra'), may hold values from 0.1 to 1.9
- second_gate: float32 [3072, 8192], P('ra', 'cb'), may hold values from -0.109375 to 0.109375
- second_up: float32 [3072, 8192], P('ra', 'cb'), may hold values from -0.109375 to 0.109375
- second_down: float32 [8192, 3072], P('cb', 'ra'), may hold values from -0.0625 to 0.0625
- second_gate_scale: float32 [8192], P('cb'), may hold values from 0.5 to 2
- second_up_scale: float32 [8192], P('cb'), may hold values from 0.5 to 2
- second_down_scale: float32 [3072], P('ra'), may hold values from 0.5 to 2
Outputs:
- mixed: bfloat16 [256, 3072], P(None, 'ra')
Inputs may be any that keep to these rules, and one draw needn't show every extreme that they name: The features come in groups of 64 with different magnitudes, and tokens differ in magnitude.
All inputs are finite; a program needn't handle non-finite values.
Results may differ from a plain program's by a relative error of at most 0.0093.
Values may be sent and summed in bfloat16 or wider, within the bound.
A program may use at most 64 MiB of HBM per device.

v0:
```python
import jax
import jax.numpy as jnp
from jax import lax
from jax.sharding import PartitionSpec as P

D = 3072


def half_step(stream_in, gain, w_gate, w_up, w_down, gate_scale, up_scale, down_scale):
    stream = stream_in.astype(jnp.float32)
    squares = jnp.sum(stream * stream, axis=1)
    shaped = (stream * gain[None, :]).astype(jnp.bfloat16)
    gate_part = jnp.dot(shaped, w_gate.astype(jnp.bfloat16), preferred_element_type=jnp.float32)
    up_part = jnp.dot(shaped, w_up.astype(jnp.bfloat16), preferred_element_type=jnp.float32)
    squares, gate_sum, up_sum = lax.psum((squares, gate_part, up_part), "ra")
    inverse = lax.rsqrt(squares / D + 1e-06)[:, None]
    gate_full = inverse * gate_scale[None, :] * gate_sum
    up_full = inverse * up_scale[None, :] * up_sum
    hidden = (jax.nn.silu(gate_full) * up_full).astype(jnp.bfloat16)
    down_part = jnp.dot(hidden, w_down.astype(jnp.bfloat16), preferred_element_type=jnp.float32)
    down_sum = lax.psum(down_part, "cb")
    return (stream + 0.5 * down_scale[None, :] * down_sum).astype(jnp.bfloat16)


def body(
    tokens,
    first_gain,
    first_gate,
    first_up,
    first_down,
    first_gate_scale,
    first_up_scale,
    first_down_scale,
    second_gain,
    second_gate,
    second_up,
    second_down,
    second_gate_scale,
    second_up_scale,
    second_down_scale,
):
    middle = half_step(
        tokens,
        first_gain,
        first_gate,
        first_up,
        first_down,
        first_gate_scale,
        first_up_scale,
        first_down_scale,
    )
    return half_step(
        middle,
        second_gain,
        second_gate,
        second_up,
        second_down,
        second_gate_scale,
        second_up_scale,
        second_down_scale,
    )


def solution(mesh):
    return jax.shard_map(
        body,
        mesh=mesh,
        in_specs=(
            P(None, "ra"),
            P("ra"),
            P("ra", "cb"),
            P("ra", "cb"),
            P("cb", "ra"),
            P("cb"),
            P("cb"),
            P("ra"),
            P("ra"),
            P("ra", "cb"),
            P("ra", "cb"),
            P("cb", "ra"),
            P("cb"),
            P("cb"),
            P("ra"),
        ),
        out_specs=P(None, "ra"),
        check_vma=False,
    )
```

profile of v0, /device:TPU:0, one launch (start us, length us, event | category | flops | bytes accessed | tf_op | source)
XLA Modules:
  0.0 416.3 jit_solution(14474829780918791749)
XLA Ops:
  6.5 4.2 %fusion.10 = f32[256,2048]{1,0:T(8,128)} fusion(f32[384,2048]{1,0:T(8,128)} %param.17, bf16[256,384]{1,0:T(8,128)(2,1)} %param.15, f32[384]{0:T(512)} %param.16), kind=kOutput, calls=%fused_computation.12 | convolution fusion | flops 403734528 | bytes 5441024 | tf_op jit(solution)/shard_map/dot_general | solution.py:13
  10.8 2.0 fusion.8
  12.8 0.0 all-reduce.13.cloned.1.call-update
  12.8 0.0 all-reduce.7.cloned.1.call-start
  12.9 0.1 fusion.12
  13.0 24.3 %psum.56 = f32[256]{0:T(256)S(1)} all-reduce(f32[256]{0:T(256)S(1)} %fusion.12), channel_id=1, replica_groups=mesh['ra'=8,'cb'=4] {'ra'}, use_global_device_ids=true, to_apply=%region_1.0 | all-reduce | flops 256 | bytes 2048 | tf_op jit(solution)/shard_map/psum | solution.py:15
  37.3 135.1 %all-reduce.13.cloned.1.call-done = (f32[256,2048]{1,0:T(8,128)}, f32[256,2048]{1,0:T(8,128)}) async-done(((f32[256,2048]{1,0:T(8,128)}, f32[256,2048]{1,0:T(8,128)}), (f32[256,2048]{1,0:T(8,128)}, f32[256,2048]{1,0:T(8,128)})) %all-reduce.13.cloned.1.call-update) | async-done | bytes 4194320 | tf_op jit(solution)/shard_map/psum | solution.py:15
  172.4 0.0 copy-start.5
  172.4 5.1 %fusion.6 = f32[256,384]{1,0:T(8,128)} fusion(f32[2048,384]{1,0:T(8,128)} %param.19, f32[256,2048]{1,0:T(8,128)} %get-tuple-element.7, f32[256,2048]{1,0:T(8,128)} %get-tuple-element.8, f32[2048]{0:T(1024)S(1)} %copy-done.9, f32[2048]{0:T(1024)S(1)} %copy-done.10, f32[256]{0:T(256)S(1)} %add_rsqrt_fusion.1), kind=kOutput, calls=%fused_computation.8 | convolution fusion | flops 408682496 | bytes 7750656 | tf_op jit(solution)/shard_map/dot_general | solution.py:20
  177.5 0.0 all-reduce.7.cloned.1.call-update
  177.6 0.0 all-reduce.11.cloned.1.call-start
  177.6 31.9 %all-reduce.7.cloned.1.call-done = f32[256,384]{1,0:T(8,128)} async-done(((f32[256,384]{1,0:T(8,128)}), f32[256,384]{1,0:T(8,128)}) %all-reduce.7.cloned.1.call-update) | async-done | bytes 393232 | tf_op jit(solution)/shard_map/psum | solution.py:21
  209.5 1.1 fusion.15
  210.7 2.0 fusion.2
  212.7 0.3 copy-done.3
  213.1 2.1 fusion.4
  215.2 0.0 all-reduce.11.cloned.1.call-update
  215.2 0.0 all-reduce.9.cloned.1.call-start
  215.2 22.8 %psum.60 = f32[256]{0:T(256)S(1)} all-reduce(f32[256]{0:T(256)S(1)} %get-tuple-element.9), channel_id=1, replica_groups=mesh['ra'=8,'cb'=4] {'ra'}, use_global_device_ids=true, to_apply=%region_6.7 | all-reduce | flops 256 | bytes 2048 | tf_op jit(solution)/shard_map/psum | solution.py:15
  238.0 133.9 %all-reduce.11.cloned.1.call-done = (f32[256,2048]{1,0:T(8,128)}, f32[256,2048]{1,0:T(8,128)}) async-done(((f32[256,2048]{1,0:T(8,128)}, f32[256,2048]{1,0:T(8,128)}), (f32[256,2048]{1,0:T(8,128)}, f32[256,2048]{1,0:T(8,128)})) %all-reduce.11.cloned.1.call-update) | async-done | bytes 4194320 | tf_op jit(solution)/shard_map/psum | solution.py:15
  372.0 4.1 fusion
  376.0 0.0 all-reduce.9.cloned.1.call-update
  376.1 31.9 %all-reduce.9.cloned.1.call-done = f32[256,384]{1,0:T(8,128)} async-done(((f32[256,384]{1,0:T(8,128)}), f32[256,384]{1,0:T(8,128)}) %all-reduce.9.cloned.1.call-update) | async-done | bytes 393232 | tf_op jit(solution)/shard_map/psum | solution.py:21
  408.0 1.7 fusion.17
  (29 shorter events, 0.1 us)
Async XLA Ops:
  6.5 4.2 %copy-start = (bf16[256,384]{1,0:T(8,128)(2,1)S(1)}, bf16[256,384]{1,0:T(8,128)(2,1)}, u32[]{:S(2)}) copy-start(bf16[256,384]{1,0:T(8,128)(2,1)} %param.15) | copy-start | bytes 589828
  6.5 4.2 %copy-start.4 = (f32[384]{0:T(512)S(1)}, f32[384]{0:T(512)}, u32[]{:S(2)}) copy-start(f32[384]{0:T(512)} %param.16) | copy-start | bytes 4612
  6.5 4.2 %copy-start.1 = (f32[384,2048]{1,0:T(8,128)S(1)}, f32[384,2048]{1,0:T(8,128)}, u32[]{:S(2)}) copy-start(f32[384,2048]{1,0:T(8,128)} %param.18) | copy-start | bytes 9437188
  6.5 165.9 %all-reduce.13.cloned.1.call-start = ((), (), s32[]{:S(2)}) async-start(), calls=%async_computation.3 | async-start | bytes 8388608 | tf_op jit(solution)/shard_map/psum | solution.py:15
  12.8 159.6 %copy-start.9 = (f32[2048]{0:T(1024)S(1)}, f32[2048]{0:T(1024)}, u32[]{:S(2)}) copy-start(f32[2048]{0:T(1024)} %param.21) | copy-start | bytes 24580
  12.8 159.6 %copy-start.10 = (f32[2048]{0:T(1024)S(1)}, f32[2048]{0:T(1024)}, u32[]{:S(2)}) copy-start(f32[2048]{0:T(1024)} %param.20) | copy-start | bytes 24580
  12.8 196.7 %all-reduce.7.cloned.1.call-start = ((), (), s32[]{:S(2)}) async-start(), calls=%async_computation | async-start | bytes 786432 | tf_op jit(solution)/shard_map/psum | solution.py:21
  172.4 5.2 %copy-start.6 = (f32[384]{0:T(512)S(1)}, f32[384]{0:T(512)}, u32[]{:S(2)}) copy-start(f32[384]{0:T(512)} %param.22) | copy-start | bytes 4612
  172.4 38.3 %copy-start.2 = (f32[384,2048]{1,0:T(8,128)S(1)}, f32[384,2048]{1,0:T(8,128)}, u32[]{:S(2)}) copy-start(f32[384,2048]{1,0:T(8,128)} %param.25) | copy-start | bytes 9437188
  172.4 38.3 %copy-start.5 = (f32[384]{0:T(512)S(1)}, f32[384]{0:T(512)}, u32[]{:S(2)}) copy-start(f32[384]{0:T(512)} %param.23) | copy-start | bytes 4612
  177.6 194.4 %all-reduce.11.cloned.1.call-start = ((), (), s32[]{:S(2)}) async-start(), calls=%async_computation.2 | async-start | bytes 8388608 | tf_op jit(solution)/shard_map/psum | solution.py:15
  210.7 2.4 copy-start.3
  215.2 156.8 %copy-start.8 = (f32[2048,384]{1,0:T(8,128)S(1)}, f32[2048,384]{1,0:T(8,128)}, u32[]{:S(2)}) copy-start(f32[2048,384]{1,0:T(8,128)} %param.26) | copy-start | bytes 9437188
  215.2 156.8 %copy-start.11 = (f32[2048]{0:T(1024)S(1)}, f32[2048]{0:T(1024)}, u32[]{:S(2)}) copy-start(f32[2048]{0:T(1024)} %param.28) | copy-start | bytes 24580
  215.2 156.8 %copy-start.12 = (f32[2048]{0:T(1024)S(1)}, f32[2048]{0:T(1024)}, u32[]{:S(2)}) copy-start(f32[2048]{0:T(1024)} %param.27) | copy-start | bytes 24580
  215.2 192.8 %all-reduce.9.cloned.1.call-start = ((), (), s32[]{:S(2)}) async-start(), calls=%async_computation.1 | async-start | bytes 786432 | tf_op jit(solution)/shard_map/psum | solution.py:21
  372.0 4.1 copy-start.7
Sparse Core Ops, SparseCore 0:
  13.0 159.4 all-reduce.12
  177.7 31.7 all-reduce.6
  215.3 156.5 all-reduce.10
  376.2 31.7 all-reduce.8
where the time goes:
time: 417 us; the launch traced here: 416 us
  waiting for transfers between devices  333 us (80%)
  blocking collectives  47 us (11%)
  matrix products  19.6 us (5%)
  between operations  13.2 us (3%)
    psum x2, waiting for transfers between devices, half_step(): squares, gate_sum, up_sum = lax.psum((squares, gate_part, up_part), 'ra')  269 us
    psum x2, waiting for transfers between devices, half_step(): down_sum = lax.psum(down_part, 'cb')  63.8 us
    psum x2, blocking collectives, half_step(): squares, gate_sum, up_sum = lax.psum((squares, gate_part, up_part), 'ra')  47 us
    dot_general x2, matrix products, half_step(): jnp.dot(hidden, w_down.astype(jnp.bfloat16), preferred_element_type=jnp.f...  9.19 us
  transfers between devices with their start and end apart: 4, of which 4 were waited for; matrix products, arithmetic and copies ran while one was open for 0% of the time, Pallas kernels for 0%

commit v1 on v0

--- a/solution.py
+++ b/solution.py
@@ -4,6 +4,11 @@
 from jax.sharding import PartitionSpec as P
 
 D = 3072
+
+
+def _compute_lots_all(xin):
+    f_now = jax.lax.all_gather(xin, axis_name="cb")
+    return jnp.sum(f_now, axis=0)
 
 
 def half_step(stream_in, gain, w_gate, w_up, w_down, gate_scale, up_scale, down_scale):
@@ -18,7 +23,7 @@
     up_full = inverse * up_scale[None, :] * up_sum
     hidden = (jax.nn.silu(gate_full) * up_full).astype(jnp.bfloat16)
     down_part = jnp.dot(hidden, w_down.astype(jnp.bfloat16), preferred_element_type=jnp.float32)
-    down_sum = lax.psum(down_part, "cb")
+    down_sum = _compute_lots_all(down_part)
     return (stream + 0.5 * down_scale[None, :] * down_sum).astype(jnp.bfloat16)
 
 

time: 417 us -> 392 us (0.940)
  waiting for transfers between devices: 333 us -> 306 us
    psum x2 -> x0, waiting for transfers between devices: 63.8 us -> none  [half_step(): down_sum = lax.psum(down_part, 'cb')]
    all_gather x0 -> x2, waiting for transfers between devices: none -> 37.5 us  [_compute_lots_all(): f_now = jax.lax.all_gather(xin, axis_name='cb')]
where the time goes in v1:
time: 392 us
  waiting for transfers between devices  306 us (78%)
  blocking collectives  47.1 us (12%)
  matrix products  18.5 us (5%)
  between operations  13.2 us (3%)
  other arithmetic  5.83 us (1%)
    psum x2, waiting for transfers between devices, half_step(): squares, gate_sum, up_sum = lax.psum((squares, gate_part, up_part), 'ra')  269 us
    psum x2, blocking collectives, half_step(): squares, gate_sum, up_sum = lax.psum((squares, gate_part, up_part), 'ra')  47.1 us
    all_gather x2, waiting for transfers between devices, _compute_lots_all(): f_now = jax.lax.all_gather(xin, axis_name='cb')  37.5 us
    dot_general x2, matrix products, half_step(): jnp.dot(hidden, w_down.astype(jnp.bfloat16), preferred_element_type=jnp.f...  8.08 us
  transfers between devices with their start and end apart: 4, of which 4 were waited for; matrix products, arithmetic and copies ran while one was open for 0% of the time, Pallas kernels for 0%

profile of v1, /device:TPU:0, one launch (start us, length us, event | category | flops | bytes accessed | tf_op | source)
XLA Modules:
  0.0 391.6 jit_solution(6429474965641833515)
XLA Ops:
  6.5 4.2 %fusion.10 = f32[256,2048]{1,0:T(8,128)} fusion(f32[384,2048]{1,0:T(8,128)} %param.17, bf16[256,384]{1,0:T(8,128)(2,1)} %param.15, f32[384]{0:T(512)} %param.16), kind=kOutput, calls=%fused_computation.12 | convolution fusion | flops 403734528 | bytes 5441024 | tf_op jit(solution)/shard_map/dot_general | solution.py:18
  10.8 2.1 fusion.8
  12.8 0.0 all-reduce.7.cloned.1.call-update
  12.9 0.0 all-gather.5.cloned.1.call-start
  12.9 0.1 fusion.12
  13.0 24.3 %psum.42 = f32[256]{0:T(256)S(1)} all-reduce(f32[256]{0:T(256)S(1)} %fusion.12), channel_id=1, replica_groups=mesh['ra'=8,'cb'=4] {'ra'}, use_global_device_ids=true, to_apply=%region_1.0 | all-reduce | flops 256 | bytes 2048 | tf_op jit(solution)/shard_map/psum | solution.py:20
  37.4 135.0 %all-reduce.7.cloned.1.call-done = (f32[256,2048]{1,0:T(8,128)}, f32[256,2048]{1,0:T(8,128)}) async-done(((f32[256,2048]{1,0:T(8,128)}, f32[256,2048]{1,0:T(8,128)}), (f32[256,2048]{1,0:T(8,128)}, f32[256,2048]{1,0:T(8,128)})) %all-reduce.7.cloned.1.call-update) | async-done | bytes 4194320 | tf_op jit(solution)/shard_map/psum | solution.py:20
  172.4 4.0 %fusion.6 = f32[256,384]{1,0:T(8,128)} fusion(f32[2048,384]{1,0:T(8,128)S(1)} %copy-done.8, f32[256,2048]{1,0:T(8,128)} %get-tuple-element.7, f32[256,2048]{1,0:T(8,128)} %get-tuple-element.8, f32[2048]{0:T(1024)S(1)} %copy-done.10, f32[2048]{0:T(1024)S(1)} %copy-done.11, f32[256]{0:T(256)S(1)} %add_rsqrt_fusion.1), kind=kOutput, calls=%fused_computation.8 | convolution fusion | flops 408682496 | bytes 7750656 | tf_op jit(solution)/shard_map/dot_general | solution.py:25
  176.4 0.0 all-gather.5.cloned.1.call-update
  176.4 0.0 all-reduce.5.cloned.1.call-start
  176.5 18.7 %all-gather.5.cloned.1.call-done = f32[1024,384]{1,0:T(8,128)} async-done(((f32[256,384]{1,0:T(8,128)}), f32[1024,384]{1,0:T(8,128)}) %all-gather.5.cloned.1.call-update) | async-done | bytes 1572880 | tf_op jit(solution)/shard_map/all_gather | solution.py:10
  195.2 2.3 reduce_sum.37
  197.5 1.1 fusion.15
  198.7 2.0 fusion.2
  200.7 0.3 copy-done.3
  201.0 2.1 fusion.4
  203.2 0.0 all-gather.7.cloned.1.call-start
  203.2 22.8 %psum.45 = f32[256]{0:T(256)S(1)} all-reduce(f32[256]{0:T(256)S(1)} %get-tuple-element.9), channel_id=1, replica_groups=mesh['ra'=8,'cb'=4] {'ra'}, use_global_device_ids=true, to_apply=%region_6.7 | all-reduce | flops 256 | bytes 2048 | tf_op jit(solution)/shard_map/psum | solution.py:20
  226.0 133.9 %all-reduce.5.cloned.1.call-done = (f32[256,2048]{1,0:T(8,128)}, f32[256,2048]{1,0:T(8,128)}) async-done(((f32[256,2048]{1,0:T(8,128)}, f32[256,2048]{1,0:T(8,128)}), (f32[256,2048]{1,0:T(8,128)}, f32[256,2048]{1,0:T(8,128)})) %all-reduce.5.cloned.1.call-update) | async-done | bytes 4194320 | tf_op jit(solution)/shard_map/psum | solution.py:20
  359.9 4.1 %fusion = f32[256,384]{1,0:T(8,128)} fusion(f32[2048,384]{1,0:T(8,128)S(1)} %copy-done.9, f32[256,2048]{1,0:T(8,128)} %get-tuple-element.5, f32[256,2048]{1,0:T(8,128)} %get-tuple-element.6, f32[2048]{0:T(1024)S(1)} %copy-done.12, f32[2048]{0:T(1024)S(1)} %copy-done.13, f32[256]{0:T(256)S(1)} %add_rsqrt_fusion), kind=kOutput, calls=%fused_computation.2 | convolution fusion | flops 408682496 | bytes 7750656 | tf_op jit(solution)/shard_map/dot_general | solution.py:25
  364.0 0.0 all-gather.7.cloned.1.call-update
  364.0 18.8 %all-gather.7.cloned.1.call-done = f32[1024,384]{1,0:T(8,128)} async-done(((f32[256,384]{1,0:T(8,128)}), f32[1024,384]{1,0:T(8,128)}) %all-gather.7.cloned.1.call-update) | async-done | bytes 1572880 | tf_op jit(solution)/shard_map/all_gather | solution.py:10
  382.8 1.5 reduce_sum.39
  384.3 0.7 fusion.17
  (33 shorter events, 0.1 us)
Async XLA Ops:
  6.5 4.2 %copy-start = (bf16[256,384]{1,0:T(8,128)(2,1)S(1)}, bf16[256,384]{1,0:T(8,128)(2,1)}, u32[]{:S(2)}) copy-start(bf16[256,384]{1,0:T(8,128)(2,1)} %param.15) | copy-start | bytes 589828
  6.5 4.2 %copy-start.4 = (f32[384]{0:T(512)S(1)}, f32[384]{0:T(512)}, u32[]{:S(2)}) copy-start(f32[384]{0:T(512)} %param.16) | copy-start | bytes 4612
  6.5 4.2 %copy-start.1 = (f32[384,2048]{1,0:T(8,128)S(1)}, f32[384,2048]{1,0:T(8,128)}, u32[]{:S(2)}) copy-start(f32[384,2048]{1,0:T(8,128)} %param.18) | copy-start | bytes 9437188
  6.5 165.8 %all-reduce.7.cloned.1.call-start = ((), (), s32[]{:S(2)}) async-start(), calls=%async_computation.3 | async-start | bytes 8388608 | tf_op jit(solution)/shard_map/psum | solution.py:20
  12.8 159.5 %copy-start.8 = (f32[2048,384]{1,0:T(8,128)S(1)}, f32[2048,384]{1,0:T(8,128)}, u32[]{:S(2)}) copy-start(f32[2048,384]{1,0:T(8,128)} %param.19) | copy-start | bytes 9437188
  12.8 159.5 %copy-start.10 = (f32[2048]{0:T(1024)S(1)}, f32[2048]{0:T(1024)}, u32[]{:S(2)}) copy-start(f32[2048]{0:T(1024)} %param.21) | copy-start | bytes 24580
  12.8 159.5 %copy-start.11 = (f32[2048]{0:T(1024)S(1)}, f32[2048]{0:T(1024)}, u32[]{:S(2)}) copy-start(f32[2048]{0:T(1024)} %param.20) | copy-start | bytes 24580
  12.9 182.3 %all-gather.5.cloned.1.call-start = ((), (), s32[]{:S(2)}) async-start(), calls=%async_computation | async-start | bytes 1966080 | tf_op jit(solution)/shard_map/all_gather | solution.py:10
  172.4 4.1 %copy-start.6 = (f32[384]{0:T(512)S(1)}, f32[384]{0:T(512)}, u32[]{:S(2)}) copy-start(f32[384]{0:T(512)} %param.22) | copy-start | bytes 4612
  176.4 22.3 %copy-start.2 = (f32[384,2048]{1,0:T(8,128)S(1)}, f32[384,2048]{1,0:T(8,128)}, u32[]{:S(2)}) copy-start(f32[384,2048]{1,0:T(8,128)} %param.25) | copy-start | bytes 9437188
  176.4 22.3 %copy-start.5 = (f32[384]{0:T(512)S(1)}, f32[384]{0:T(512)}, u32[]{:S(2)}) copy-start(f32[384]{0:T(512)} %param.23) | copy-start | bytes 4612
  176.4 183.5 %all-reduce.5.cloned.1.call-start = ((), (), s32[]{:S(2)}) async-start(), calls=%async_computation.2 | async-start | bytes 8388608 | tf_op jit(solution)/shard_map/psum | solution.py:20
  198.7 2.4 copy-start.3
  203.1 156.8 %copy-start.9 = (f32[2048,384]{1,0:T(8,128)S(1)}, f32[2048,384]{1,0:T(8,128)}, u32[]{:S(2)}) copy-start(f32[2048,384]{1,0:T(8,128)} %param.26) | copy-start | bytes 9437188
  203.1 156.8 %copy-start.12 = (f32[2048]{0:T(1024)S(1)}, f32[2048]{0:T(1024)}, u32[]{:S(2)}) copy-start(f32[2048]{0:T(1024)} %param.28) | copy-start | bytes 24580
  203.1 156.8 %copy-start.13 = (f32[2048]{0:T(1024)S(1)}, f32[2048]{0:T(1024)}, u32[]{:S(2)}) copy-start(f32[2048]{0:T(1024)} %param.27) | copy-start | bytes 24580
  203.2 179.7 %all-gather.7.cloned.1.call-start = ((), (), s32[]{:S(2)}) async-start(), calls=%async_computation.1 | async-start | bytes 1966080 | tf_op jit(solution)/shard_map/all_gather | solution.py:10
  359.9 4.1 %copy-start.7 = (f32[384]{0:T(512)S(1)}, f32[384]{0:T(512)}, u32[]{:S(2)}) copy-start(f32[384]{0:T(512)} %param.29) | copy-start | bytes 4612
Sparse Core Ops, SparseCore 0:
  13.0 159.3 all-reduce.6
  176.5 18.6 all-gather.4
  203.3 156.5 all-reduce.4
  364.1 18.6 all-gather.6
